TPU v7x, 32 devices: a whole 2x2x4 slice. The times are simulated.
32 devices in a mesh: sp: 16 (over z, y, x), tp: 2 (over core).
Axes of the slice: x: 2, y: 2, z: 4, core: 2. Of those that a mesh axis runs over, the one named last changes fastest.
Arguments:
- stream_signals: bfloat16 [2048, 1024], P('sp', 'tp'), may hold values from -6 to 6
- cluster_entry_matrices: bfloat16 [2048, 256], P('sp', 'tp'), may hold values from -6 to 6
- cluster_exit_matrices: bfloat16 [2048, 256], P('sp', 'tp'), may hold values from -6 to 6
- valve_logits: bfloat16 [2048, 1024], P('sp', 'tp'), may hold values from -12 to 12
- stride_logits: bfloat16 [2048, 16], P('sp', 'tp'), may hold values from -2.7 to 2.7
- surplus_log_fading: float32 [2048, 16], P('sp', 'tp'), may hold values from -0.69 to 0
- stream_filter_coefficients: bfloat16 [4, 1024], P(None, 'tp'), may hold values from -3 to 3
- entry_filter_coefficients: bfloat16 [4, 256], P(None, 'tp'), may hold values from -3 to 3
- exit_filter_coefficients: bfloat16 [4, 256], P(None, 'tp'), may hold values from -3 to 3
- stride_offset_vector: float32 [16], P('tp'), may hold values from -3.3 to 1.3
- channel_fading_speed: float32 [16], P('tp'), may hold values from 0 to 0.03
- rescale_amplitude: bfloat16 [1024], P('tp'), may hold values from 0.099609375 to 1.8984375
- final_linear_matrix: bfloat16 [1024, 2048], P('tp'), may hold values from -0.1875 to 0.1875
Outputs:
- merged: bfloat16 [2048, 2048], P(('sp', 'tp'))
All inputs are finite; a program needn't handle non-finite values.
Results may differ from a plain program's by a relative error of at most 0.013.
Values may be sent and summed in bfloat16 or wider, within the bound.
A program may use at most 128 MiB of HBM per device.

v0:
```python
import jax
import jax.numpy as jnp
from jax import lax
from jax.sharding import PartitionSpec as P

HEAD_DIM = 64
STATE = 64


EPS = 1e-05
FULL_PRECISION = lax.Precision.HIGHEST


def from_behind(value, axis, steps):
    count = lax.axis_size(axis)
    first, last = (max(0, -steps), min(count, count - steps))
    return lax.ppermute(value, axis, [(source, source + steps) for source in range(first, last)])


def carried_in(array, axis, join, neutral):
    place = lax.axis_index(axis)
    gathered = jax.tree.map(
        lambda a, kind: lax.all_gather(a.astype(kind), axis),
        array,
        jax.tree.map(lambda a: jnp.bfloat16 if a.dtype == jnp.float32 else a.dtype, array),
    )
    state = jax.tree.map(lambda a, e: jnp.zeros_like(a) + jnp.asarray(e, a.dtype), array, neutral)

    def one(turn, state):
        return join(
            state,
            jax.tree.map(
                lambda a, own: lax.dynamic_index_in_dim(a, turn, 0, False).astype(own.dtype),
                gathered,
                array,
            ),
        )

    return lax.fori_loop(0, place, one, state)


def conv_silu(signal, prior, kernel):
    length = signal.shape[0]
    joined = jnp.concatenate([prior, signal], axis=0).astype(jnp.float32)
    taps = kernel.astype(jnp.float32)
    summed = jnp.zeros(signal.shape, jnp.float32)
    for offset in range(kernel.shape[0]):
        summed = summed + taps[offset] * joined[offset : offset + length]
    return jax.nn.silu(summed).astype(jnp.bfloat16)


def block_terms(conv_x, conv_b, conv_c, stride_length, within_segment):
    length = conv_x.shape[0]
    groups = conv_b.shape[1] // STATE
    head_count = stride_length.shape[1]
    per_group = head_count // groups
    b_heads = conv_b.reshape(length, groups, STATE)
    c_heads = conv_c.reshape(length, groups, STATE)
    x_scaled = (
        conv_x.astype(jnp.float32).reshape(length, head_count, HEAD_DIM) * stride_length[:, :, None]
    ).astype(jnp.bfloat16)
    scores = jnp.einsum("tgn,sgn->gts", c_heads, b_heads, preferred_element_type=jnp.float32)
    gap_log = within_segment.T[:, :, None] - within_segment.T[:, None, :]
    causal = lax.iota(jnp.int32, length)[:, None] >= lax.iota(jnp.int32, length)[None, :]
    decays = jnp.exp(jnp.where(causal[None], gap_log, -jnp.inf)).reshape(
        groups, per_group, length, length
    )
    decay_weights = (scores[:, None] * decays).astype(jnp.bfloat16)
    head_input_rows = x_scaled.reshape(length, groups, per_group, HEAD_DIM)
    intra_block_term = jnp.einsum(
        "wbzv,vwbi->zwbi", decay_weights, head_input_rows, preferred_element_type=jnp.float32
    )
    block_decay = within_segment[-1]
    to_end = jnp.exp(block_decay[None] - within_segment).reshape(length, groups, per_group)
    b_end = (to_end[..., None] * b_heads.astype(jnp.float32)[:, :, None, :]).astype(jnp.bfloat16)
    block_state = jnp.einsum(
        "sgrp,sgrn->grpn", head_input_rows, b_end, preferred_element_type=jnp.float32
    )
    growth = jnp.exp(within_segment).reshape(length, groups, per_group)
    return (
        intra_block_term,
        block_state,
        block_decay.reshape(groups, per_group),
        c_heads.astype(jnp.float32),
        growth,
    )


def read_state(c_heads, growth, entering):
    return growth[..., None] * jnp.einsum(
        "tgn,grpn->tgrp", c_heads, entering, precision=FULL_PRECISION
    )


def combine(earlier, later):
    return (earlier[0] + later[0], jnp.exp(later[0])[:, :, None, None] * earlier[1] + later[1])


def per_device(
    stream_signals,
    cluster_entry_matrices,
    cluster_exit_matrices,
    valve_logits,
    stride_logits,
    surplus_log_fading,
    stream_filter_coefficients,
    entry_filter_coefficients,
    exit_filter_coefficients,
    stride_offset_vector,
    channel_fading_speed,
    rescale_amplitude,
    final_linear_matrix,
):
    rim_rows = stream_filter_coefficients.shape[0] - 1
    inner_local = stream_signals.shape[1]
    group_cols = cluster_entry_matrices.shape[1]
    length = stream_signals.shape[0]
    edge_rows = jnp.concatenate(
        [
            stream_signals[length - rim_rows :],
            cluster_entry_matrices[length - rim_rows :],
            cluster_exit_matrices[length - rim_rows :],
        ],
        axis=1,
    )
    prior_rows = from_behind(edge_rows, "sp", 1)
    conv_x = conv_silu(stream_signals, prior_rows[:, :inner_local], stream_filter_coefficients)
    conv_b = conv_silu(
        cluster_entry_matrices,
        prior_rows[:, inner_local : inner_local + group_cols],
        entry_filter_coefficients,
    )
    conv_c = conv_silu(
        cluster_exit_matrices, prior_rows[:, inner_local + group_cols :], exit_filter_coefficients
    )
    stride_length = jax.nn.softplus(stride_logits.astype(jnp.float32) + stride_offset_vector[None])
    within_segment = jnp.cumsum(
        surplus_log_fading - stride_length * channel_fading_speed[None], axis=0
    )
    intra_block_term, block_state, block_decay, c_heads, growth = block_terms(
        conv_x, conv_b, conv_c, stride_length, within_segment
    )
    pair = (block_decay, block_state)
    entering = carried_in(pair, "sp", combine, jax.tree.map(jnp.zeros_like, pair))[1]
    readout = read_state(c_heads, growth, entering)
    values = (intra_block_term + readout).reshape(length, inner_local)
    gated = values * jax.nn.silu(valve_logits.astype(jnp.float32))
    ways = lax.axis_size("tp")
    regrouped = lax.all_to_all(
        gated.astype(jnp.bfloat16), "tp", split_axis=0, concat_axis=1, tiled=True
    ).astype(gated.dtype)
    whole_weight, whole_gain = (
        lax.all_gather(final_linear_matrix, "tp", axis=0, tiled=True),
        lax.all_gather(rescale_amplitude, "tp", axis=0, tiled=True),
    )
    scale = lax.rsqrt(jnp.mean(regrouped * regrouped, axis=1) + EPS)
    normed = (regrouped * scale[:, None] * whole_gain.astype(jnp.float32)[None]).astype(
        jnp.bfloat16
    )
    part_width = normed.shape[1] // ways
    summed = jnp.zeros((normed.shape[0], whole_weight.shape[1]), jnp.float32)
    for member in range(ways):
        portion = jnp.dot(
            normed[:, member * part_width : (member + 1) * part_width],
            whole_weight[member * part_width : (member + 1) * part_width],
            preferred_element_type=jnp.float32,
        ).astype(jnp.bfloat16)
        summed = summed + portion.astype(jnp.float32)
    return summed.astype(jnp.bfloat16)


def solution(mesh):
    placed = (
        P("sp", "tp"),
        P("sp", "tp"),
        P("sp", "tp"),
        P("sp", "tp"),
        P("sp", "tp"),
        P("sp", "tp"),
        P(None, "tp"),
        P(None, "tp"),
        P(None, "tp"),
        P("tp"),
        P("tp"),
        P("tp"),
        P("tp", None),
    )
    return jax.shard_map(
        per_device, mesh=mesh, in_specs=placed, out_specs=P(("sp", "tp"), None), check_vma=False
    )
```

profile of v0, /device:TPU:31, one launch (start us, length us, event | category | flops | bytes accessed | tf_op | source)
XLA Modules:
  0.0 111.9 jit_solution(1617715553484355451)
XLA Ops:
  8.8 1.3 %collective-permute-start = (bf16[3,768]{0,1:T(8,128)(2,1)S(1)}, bf16[3,768]{0,1:T(8,128)(2,1)S(1)}, u32[]{:S(2)}, u32[]{:S(2)}) collective-permute-start(bf16[3,768]{0,1:T(8,128)(2,1)S(1)} %copy.46), channel_id=1, source_target_pairs={{0,2},{2,4},{4,6},{6,8},{8,10},{10,12},{12,14},{14,16},{16,18},{18... | collective-permute-start | bytes 13832 | tf_op jit(solution)/shard_map/ppermute | solution.py:17
  14.7 1.0 copy.47
  19.6 3.0 %all-gather.1 = bf16[2,1,512]{2,1,0:T(2,128)(2,1)S(1)} all-gather(bf16[1,1,512]{2,1,0:T(2,128)(2,1)S(1)} %reshape.107), channel_id=1, replica_groups=mesh['sp'=16,'tp'=2] {'tp'}, dimensions={0}, use_global_device_ids=true | all-gather | bytes 3072 | tf_op jit(solution)/shard_map/all_gather | solution.py:154
  22.6 28.3 %all_gather.16 = bf16[16,2,4]{2,1,0:T(2,128)(2,1)S(1)} all-gather(bf16[1,2,4]{2,1,0:T(2,128)(2,1)S(1)} %convert_element_type.134), channel_id=1, replica_groups=mesh['sp'=16,'tp'=2] {'sp'}, dimensions={0}, use_global_device_ids=true | all-gather | bytes 272 | tf_op jit(solution)/shard_map/all_gather | solution.py:23
  51.3 26.4 %all-gather.7.cloned.1.call-done = bf16[32,4,64,64]{3,2,1,0:T(8,128)(2,1)} async-done(((bf16[2,4,64,64]{3,2,1,0:T(8,128)(2,1)}), bf16[32,4,64,64]{3,2,1,0:T(8,128)(2,1)}) %all-gather.7.cloned.1.call-update) | async-done | bytes 1048592 | tf_op jit(solution)/shard_map/all_gather | solution.py:23
  77.7 16.1 %while.12 = (s32[]{:T(128)}, f32[2,4,64,64]{3,2,1,0:T(8,128)S(1)}, s32[]{:T(128)}, bf16[16,2,4]{2,1,0:T(2,128)(2,1)S(1)}, bf16[16,2,4,64,64]{4,3,2,1,0:T(8,128)(2,1)}, /*index=5*/s32[]{:T(128)}, s32[]{:T(128)}, s32[]{:T(128)}) while((s32[]{:T(128)}, f32[2,4,64,64]{3,2,1,0:T(8,128)S(1)}, s32[]{:T(128)}, bf16[16,2,4]{2,1,0:T(2,128)(2,1)S(1)}, ...), condition=%wide.region_2.3_spmd, body=%wide.region_1.2_spmd.sunk | while | flops 98317 | bytes 327887 | solution.py:39
  77.8 1.0 convert_add_fusion.2
  78.8 1.0 convert_add_fusion.2
  79.9 1.0 convert_add_fusion.2
  81.0 1.0 convert_add_fusion.2
  82.0 1.0 convert_add_fusion.2
  83.1 1.0 convert_add_fusion.2
  84.1 1.0 convert_add_fusion.2
  85.2 1.0 convert_add_fusion.2
  86.3 1.0 convert_add_fusion.2
  87.3 1.0 convert_add_fusion.2
  88.4 1.0 convert_add_fusion.2
  89.5 1.1 convert_add_fusion.2
  90.6 1.1 convert_add_fusion.2
  91.7 1.0 convert_add_fusion.2
  92.8 1.0 convert_add_fusion.2
  94.7 5.2 %all_to_all.13 = bf16[2,64,512]{2,1,0:T(8,128)(2,1)S(1)} all-to-all(bf16[2,64,512]{2,1,0:T(8,128)(2,1)S(1)} %bitcast.68), channel_id=1, replica_groups=mesh['sp'=16,'tp'=2] {'tp'}, dimensions={0} | all-to-all | bytes 262144 | tf_op jit(solution)/shard_map/all_to_all | solution.py:149
  100.2 2.1 %fusion.3 = f32[64,2048]{1,0:T(8,128)S(1)} fusion(bf16[1024,2048]{1,0:T(8,128)(2,1)} %all-gather.5.cloned.1.call-done, bf16[64,1024]{1,0:T(8,128)(2,1)S(1)} %multiply_convert_fusion.2), kind=kOutput, calls=%fused_computation.7 | convolution fusion | flops 134479872 | bytes 2686976 | tf_op jit(solution)/shard_map/dot_general | solution.py:163
  102.3 2.8 %fusion.2 = bf16[64,2048]{1,0:T(8,128)(2,1)} fusion(f32[64,2048]{1,0:T(8,128)S(1)} %fusion.3, bf16[1024,2048]{1,0:T(8,128)(2,1)} %all-gather.5.cloned.1.call-done, bf16[64,1024]{1,0:T(8,128)(2,1)S(1)} %multiply_convert_fusion.2), kind=kOutput, calls=%fused_computation.5 | convolution fusion | flops 134742016 | bytes 2949120 | tf_op jit(solution)/shard_map/dot_general | solution.py:163
  (73 shorter events, 12.3 us)
Async XLA Ops:
  6.5 71.2 %all-gather.7.cloned.1.call-start = ((), (), s32[]{:S(2)}) async-start(), calls=%async_computation.2 | async-start | bytes 2228224 | tf_op jit(solution)/shard_map/all_gather | solution.py:23
  8.8 7.7 %collective-permute-start = (bf16[3,768]{0,1:T(8,128)(2,1)S(1)}, bf16[3,768]{0,1:T(8,128)(2,1)S(1)}, u32[]{:S(2)}, u32[]{:S(2)}) collective-permute-start(bf16[3,768]{0,1:T(8,128)(2,1)S(1)} %copy.46), channel_id=1, source_target_pairs={{0,2},{2,4},{4,6},{6,8},{8,10},{10,12},{12,14},{14,16},{16,18},{18... | collective-permute-start | bytes 13832 | tf_op jit(solution)/shard_map/ppermute | solution.py:17
  16.8 2.5 %copy-start.1 = (bf16[4,128]{1,0:T(4,128)(2,1)S(1)}, bf16[4,128]{1,0:T(4,128)(2,1)}, u32[]{:S(2)}) copy-start(bf16[4,128]{1,0:T(4,128)(2,1)} %param.23) | copy-start | bytes 3076
  17.0 2.4 %copy-start = (bf16[128,512]{1,0:T(8,128)(2,1)S(1)}, bf16[128,512]{1,0:T(8,128)(2,1)}, u32[]{:S(2)}) copy-start(bf16[128,512]{1,0:T(8,128)(2,1)} %param.18) | copy-start | bytes 393220
  17.0 2.5 %copy-start.2 = (bf16[512]{0:T(512)(128)(2,1)S(1)}, bf16[512]{0:T(512)(128)(2,1)}, u32[]{:S(2)}) copy-start(bf16[512]{0:T(512)(128)(2,1)} %param.26) | copy-start | bytes 3076
  18.5 81.7 %all-gather.5.cloned.1.call-start = ((), (), s32[]{:S(2)}) async-start(), calls=%async_computation.1 | async-start | bytes 6291456 | tf_op jit(solution)/shard_map/all_gather | solution.py:153
Sparse Core Ops, SparseCore 0:
  18.6 59.0 all-gather.6
  79.2 16.2 all-gather.4
where the time goes:
time: 113 us; the launch traced here: 112 us
  blocking collectives  36.5 us (32%)
  waiting for transfers between devices  27.8 us (25%)
  other arithmetic  18.9 us (17%)
  between operations  13.6 us (12%)
  local copies, waits for them, and re-layouts  6.63 us (6%)
  matrix products  6.54 us (6%)
  starting transfers between devices  1.34 us (1%)
    all_gather x1, blocking collectives, carried_in(): lax.all_gather(a.astype(kind), axis)  28.3 us
    all_gather x1, waiting for transfers between devices, carried_in(): lax.all_gather(a.astype(kind), axis)  26.4 us
    add x15, other arithmetic, combine(): jnp.exp(later[0])[:, :, None, None] * earlier[1] + later[1]  15.4 us
    all_to_all x1, blocking collectives, per_device(): lax.all_to_all(gated.astype(jnp.bfloat16), 'tp', split_axis=0, concat_axi...  5.22 us
    dot_general x2, matrix products, per_device(): jnp.dot(normed[:, member * part_width:(member + 1) * part_width], whole_w...  4.85 us
    all_gather x1, blocking collectives, per_device(): lax.all_gather(rescale_amplitude, 'tp', axis=0, tiled=True)  3.02 us
    unnamed x11, local copies, waits for them, and re-layouts  2.93 us
  transfers between devices with their start and end apart: 3, of which 2 were waited for; matrix products, arithmetic and copies ran while one was open for 21% of the time, Pallas kernels for 0%

commit v1 on v0

v1 whole, which is shorter than its diff:
```python
import functools

import jax
import jax.numpy as jnp
from jax import lax
from jax.experimental import pallas as pl
from jax.experimental.pallas import tpu as pltpu
from jax.sharding import PartitionSpec as P

HEAD_DIM = 64
STATE = 64
LANES = 128
EPS = 1e-05
EXACT = lax.Precision.HIGHEST
MESH = pl.DeviceIdType.MESH
F32 = jnp.float32
BF16 = jnp.bfloat16


def silu(v):
    return v / (1.0 + jnp.exp(-v))


def kernel(
    n, owners,
    x_ref, b_ref, c_ref, z_hbm, dt_ref, fade_ref, tx_ref, tb_ref, tc_ref,
    off_ref, speed_ref, gain_ref, w_hbm,
    out_ref,
    z_ref, w_ref, halo_x, halo_b, halo_c, joined, xs, xe, cb, cc, step_e, end_e, grow_e,
    gate, y_in, dec, dec_in, st, st_in, eb, ent, gg, ssq, ssq_in, p_out, p_in,
    loc_sem, hs, hr, ds_, dr, s1, r1, s2, r2, sx, rx,
):
    length, inner = x_ref.shape
    gw = b_ref.shape[1]
    heads = dt_ref.shape[0]
    tiles = inner // LANES
    per_group_tiles = tiles // (gw // STATE)
    stride = n // owners
    rows = tiles * STATE // owners
    taps = tx_ref.shape[0]
    half = length // 2
    chunks, _, cols = p_out.shape
    me = lax.axis_index("sp")
    core = lax.axis_index("tp")
    mate = 1 - core

    z_copy = pltpu.make_async_copy(z_hbm, z_ref, loc_sem.at[0])
    w_copy = pltpu.make_async_copy(w_hbm, w_ref, loc_sem.at[1])
    z_copy.start()
    w_copy.start()

    barrier = pltpu.get_barrier_semaphore()

    def greet(i, carry):
        pl.semaphore_signal(
            barrier, inc=1, device_id={"sp": lax.rem(me + i, n)}, device_id_type=MESH
        )
        return carry

    lax.fori_loop(1, n, greet, 0)
    pl.semaphore_signal(barrier, inc=1, device_id={"tp": mate}, device_id_type=MESH)

    sub = lax.broadcasted_iota(jnp.int32, (heads, length), 0)
    off = jnp.zeros((heads, length), F32)
    speed = jnp.zeros((heads, length), F32)
    for h in range(heads):
        off = jnp.where(sub == h, off_ref[h], off)
        speed = jnp.where(sub == h, speed_ref[h], speed)
    v = dt_ref[...].astype(F32) + off
    step_t = jnp.maximum(v, 0.0) + jnp.log1p(jnp.exp(-jnp.abs(v)))
    log_t = fade_ref[...] - step_t * speed
    r_i = lax.broadcasted_iota(jnp.int32, (length, length), 0)
    c_i = lax.broadcasted_iota(jnp.int32, (length, length), 1)
    causal = r_i >= c_i
    lower = causal.astype(F32)
    eye = (r_i == c_i).astype(F32)
    nt = (((1,), (1,)), ((), ()))
    within = lax.dot_general(lower, log_t, nt, precision=EXACT, preferred_element_type=F32)
    step = lax.dot_general(eye, step_t, nt, precision=EXACT, preferred_element_type=F32)
    within_t = lax.dot_general(log_t, lower, nt, precision=EXACT, preferred_element_type=F32)
    spread = (
        lax.broadcasted_iota(jnp.int32, (heads, inner), 0)
        == lax.broadcasted_iota(jnp.int32, (heads, inner), 1) // HEAD_DIM
    ).astype(F32)
    step_e[...] = jnp.dot(step, spread, precision=EXACT, preferred_element_type=F32)
    within_e = jnp.dot(within, spread, precision=EXACT, preferred_element_type=F32)
    last = within_e[length - 1 :]
    end_e[...] = jnp.exp(last - within_e)
    grow_e[...] = jnp.exp(within_e)
    whole = jnp.exp(last)
    for t in range(tiles):
        dec[t] = whole[:, t * LANES : (t + 1) * LANES]

    lead = 8
    joined[:lead] = jnp.zeros((lead, inner + 2 * gw), F32)
    joined[lead:, :inner] = x_ref[...].astype(F32)
    joined[lead:, inner : inner + gw] = b_ref[...].astype(F32)
    joined[lead:, inner + gw :] = c_ref[...].astype(F32)

    def conv(tap_ref, first, width, start, count):
        coef = tap_ref[...].astype(F32)
        total = jnp.zeros((count, width), F32)
        for k in range(taps):
            begin = lead - (taps - 1) + k + start
            total += coef[k : k + 1] * joined[begin : begin + count, first : first + width]
        return silu(total).astype(BF16)

    def mixed(start, count):
        where = slice(start, start + count)
        scaled = conv(tx_ref, 0, inner, start, count).astype(F32) * step_e[where]
        xs[where] = scaled.astype(BF16)
        xe[where] = (scaled * end_e[where]).astype(BF16)
        cb[where] = conv(tb_ref, inner, gw, start, count)
        cc[where] = conv(tc_ref, inner + gw, gw, start, count)

    mixed(0, length)

    pl.semaphore_wait(barrier, n)

    edge = halo_x.shape[0]
    halos = [
        pltpu.make_async_remote_copy(
            src_ref=src.at[pl.ds(length - edge, edge)],
            dst_ref=dst,
            send_sem=hs.at[i],
            recv_sem=hr.at[i],
            device_id={"sp": lax.rem(me + 1, n)},
            device_id_type=MESH,
        )
        for i, (src, dst) in enumerate(((x_ref, halo_x), (b_ref, halo_b), (c_ref, halo_c)))
    ]

    @pl.when(me < n - 1)
    def _():
        for copy in halos:
            copy.start()

    base = me // stride
    tile_of = owners // tiles

    def dec_copy(owner, slot):
        return pltpu.make_async_remote_copy(
            src_ref=dec.at[owner // tile_of],
            dst_ref=dec_in.at[slot],
            send_sem=ds_.at[owner],
            recv_sem=dr.at[slot],
            device_id={"sp": owner * stride},
            device_id_type=MESH,
        )

    def st_copy(owner, slot):
        return pltpu.make_async_remote_copy(
            src_ref=st.at[owner],
            dst_ref=st_in.at[slot],
            send_sem=s1.at[owner],
            recv_sem=r1.at[slot],
            device_id={"sp": owner * stride},
            device_id_type=MESH,
        )

    def ent_copy(place, slot):
        return pltpu.make_async_remote_copy(
            src_ref=eb.at[place],
            dst_ref=ent.at[slot],
            send_sem=s2.at[place],
            recv_sem=r2.at[slot],
            device_id={"sp": place},
            device_id_type=MESH,
        )

    def to_owners(make, method, slot):
        def body(i, carry):
            owner = lax.rem(base + i, owners)

            @pl.when(owner * stride != me)
            def _():
                getattr(make(owner, slot), method)()

            return carry

        lax.fori_loop(0, owners, body, 0)

    is_owner = lax.rem(me, stride) == 0
    to_owners(dec_copy, "start", me)

    @pl.when(is_owner)
    def _():
        dec_in[me] = dec[base // tile_of]

    @pl.when(me > 0)
    def _():
        for copy in halos:
            copy.wait_recv()
        joined[:lead, :inner] = halo_x[...].astype(F32)[edge - lead :]
        joined[:lead, inner : inner + gw] = halo_b[...].astype(F32)[edge - lead :]
        joined[:lead, inner + gw :] = halo_c[...].astype(F32)[edge - lead :]
        mixed(0, 16)

    cb_t = cb[...].astype(F32).T.astype(BF16)
    per_tile = STATE // rows
    for t in range(tiles):
        g = t // per_group_tiles
        s = jnp.dot(
            cb_t[g * STATE : (g + 1) * STATE],
            xe[:, t * LANES : (t + 1) * LANES],
            preferred_element_type=F32,
        )
        for j in range(per_tile):
            st[t * per_tile + j] = s[j * rows : (j + 1) * rows].astype(BF16)

    to_owners(st_copy, "start", me)

    @pl.when(is_owner)
    def _():
        st_in[me] = st[base]

    low_lanes = lax.broadcasted_iota(jnp.int32, (length, LANES), 1) < HEAD_DIM
    for t in range(tiles):
        g = t // per_group_tiles
        if t % per_group_tiles == 0:
            scores = jnp.dot(
                cc[:, g * STATE : (g + 1) * STATE],
                cb_t[g * STATE : (g + 1) * STATE],
                preferred_element_type=F32,
            )
        parts = []
        for h in (2 * t, 2 * t + 1):
            gap = within[:, h : h + 1] - within_t[h : h + 1]
            weight = (scores * jnp.exp(jnp.where(causal, gap, -jnp.inf))).astype(BF16)
            parts.append(
                jnp.dot(
                    weight, xs[:, t * LANES : (t + 1) * LANES], preferred_element_type=F32
                )
            )
        y_in[:, t * LANES : (t + 1) * LANES] = jnp.where(low_lanes, parts[0], parts[1])
    z_copy.wait()
    gate[...] = silu(z_ref[...].astype(F32))

    @pl.when(is_owner)
    def _():
        def turn(k, state):
            @pl.when(k != me)
            def _():
                dec_copy(base, k).wait_recv()
                st_copy(base, k).wait_recv()

            eb[k] = state.astype(BF16)
            return dec_in[k] * state + st_in[k].astype(F32)

        lax.fori_loop(0, n, turn, jnp.zeros((rows, LANES), F32))

        def deliver(i, carry):
            ent_copy(lax.rem(me + i, n), base).start()
            return carry

        lax.fori_loop(1, n, deliver, 0)
        ent[base] = eb[me]

    def arrive(owner, carry):
        @pl.when(owner * stride != me)
        def _():
            ent_copy(me, owner).wait_recv()

        return carry

    lax.fori_loop(0, owners, arrive, 0)

    total = jnp.zeros((length, 1), F32)
    for t in range(tiles):
        g = t // per_group_tiles
        lanes = slice(t * LANES, (t + 1) * LANES)
        held = ent[t * per_tile : (t + 1) * per_tile].reshape(STATE, LANES)
        read = jnp.dot(cc[:, g * STATE : (g + 1) * STATE], held, preferred_element_type=F32)
        gated = (y_in[:, lanes] + grow_e[:, lanes] * read) * gate[:, lanes]
        total += jnp.sum(gated * gated, axis=1, keepdims=True)
        gg[:, lanes] = (gated * gain_ref[:, lanes].astype(F32)).astype(BF16)
    ssq[...] = jnp.broadcast_to(total, (length, LANES))

    def mate_copy(src, dst, i):
        return pltpu.make_async_remote_copy(
            src_ref=src,
            dst_ref=dst,
            send_sem=sx.at[i],
            recv_sem=rx.at[i],
            device_id={"tp": mate},
            device_id_type=MESH,
        )

    theirs = pl.ds(pl.multiple_of(mate * half, half), half)
    mine = pl.ds(pl.multiple_of(core * half, half), half)
    w_copy.wait()
    sent = []
    for i in range(chunks):
        p_out[i] = jnp.dot(
            gg[theirs], w_ref[:, i * cols : (i + 1) * cols], preferred_element_type=F32
        ).astype(BF16)
        if i == 0:
            first = mate_copy(ssq.at[theirs], ssq_in, chunks)
            first.start()
        copy = mate_copy(p_out.at[i], p_in.at[i], i)
        copy.start()
        sent.append(copy)
    own = [
        jnp.dot(gg[mine], w_ref[:, i * cols : (i + 1) * cols], preferred_element_type=F32)
        for i in range(chunks)
    ]
    first.wait_recv()
    mean = (ssq[mine] + ssq_in[...]) * (1.0 / (2 * inner))
    scale = lax.rsqrt(mean + EPS)[:, :1]
    for i in range(chunks):
        sent[i].wait_recv()
        out_ref[:, i * cols : (i + 1) * cols] = (
            (own[i] + p_in[i].astype(F32)) * scale
        ).astype(BF16)

    @pl.when(me < n - 1)
    def _():
        for copy in halos:
            copy.wait_send()

    to_owners(dec_copy, "wait_send", me)
    to_owners(st_copy, "wait_send", me)

    @pl.when(is_owner)
    def _():
        def sent_one(i, carry):
            ent_copy(lax.rem(me + i, n), base).wait_send()
            return carry

        lax.fori_loop(1, n, sent_one, 0)

    first.wait_send()
    for copy in sent:
        copy.wait_send()


def per_device(n, x, b, c, z, dt, fade, tx, tb, tc, off, speed, gain, w):
    length, inner = x.shape
    gw = b.shape[1]
    width = w.shape[1]
    tiles = inner // LANES
    owners = min(n, tiles * STATE // 16)
    rows = tiles * STATE // owners
    half = length // 2
    chunks = 4
    cols = width // chunks
    vmem = pl.BlockSpec(memory_space=pltpu.VMEM)
    smem = pl.BlockSpec(memory_space=pltpu.SMEM)
    hbm = pl.BlockSpec(memory_space=pl.ANY)
    V = pltpu.VMEM
    dma = lambda k: pltpu.SemaphoreType.DMA((k,))
    return pl.pallas_call(
        functools.partial(kernel, n, owners),
        out_shape=jax.ShapeDtypeStruct((half, width), BF16),
        in_specs=[vmem, vmem, vmem, hbm, vmem, vmem, vmem, vmem, vmem, smem, smem, vmem, hbm],
        out_specs=vmem,
        scratch_shapes=[
            V((length, inner), BF16),
            V(w.shape, BF16),
            V((16, inner), BF16),
            V((16, gw), BF16),
            V((16, gw), BF16),
            V((length + 8, inner + 2 * gw), F32),
            V((length, inner), BF16),
            V((length, inner), BF16),
            V((length, gw), BF16),
            V((length, gw), BF16),
            V((length, inner), F32),
            V((length, inner), F32),
            V((length, inner), F32),
            V((length, inner), F32),
            V((length, inner), F32),
            V((tiles, 1, LANES), F32),
            V((n, 1, LANES), F32),
            V((owners, rows, LANES), BF16),
            V((n, rows, LANES), BF16),
            V((n, rows, LANES), BF16),
            V((owners, rows, LANES), BF16),
            V((length, inner), BF16),
            V((length, LANES), F32),
            V((half, LANES), F32),
            V((chunks, half, cols), BF16),
            V((chunks, half, cols), BF16),
            dma(2), dma(3), dma(3), dma(owners), dma(n), dma(owners), dma(n),
            dma(n), dma(owners), dma(chunks + 1), dma(chunks + 1),
        ],
        compiler_params=pltpu.CompilerParams(collective_id=0, has_side_effects=True),
    )(x, b, c, z, dt.T, fade.T, tx, tb, tc, off, speed, gain.reshape(1, inner), w)


def solution(mesh):
    both = P("sp", "tp")
    taps = P(None, "tp")
    placed = (both,) * 6 + (taps,) * 3 + (P("tp"),) * 3 + (P("tp", None),)
    return jax.shard_map(
        functools.partial(per_device, mesh.shape["sp"]),
        mesh=mesh,
        in_specs=placed,
        out_specs=P(("sp", "tp"), None),
        check_vma=False,
    )
```

time: 113 us -> 27.6 us (0.24)
  the two profiles are of different devices: /device:TPU:31 before, /device:TPU:1 now
where the time goes in v1:
time: 27.6 us; the launch traced here: 27.4 us
  Pallas kernels  24.5 us (89%)
  local copies, waits for them, and re-layouts  2.93 us (11%)
    pallas_call x1, Pallas kernels, per_device(): pl.pallas_call(functools.partial(kernel, n, owners), out_shape=jax.ShapeD...  24.5 us
    unnamed x1, local copies, waits for them, and re-layouts  1.67 us
    reshape x1, local copies, waits for them, and re-layouts, per_device(): gain.reshape(1, inner)  1.26 us

profile of v1, /device:TPU:1, one launch (start us, length us, event | category | flops | bytes accessed | tf_op | source)
XLA Modules:
  0.0 27.4 jit_solution(9963864879486582752)
XLA Ops:
  0.0 1.3 %reshape.3.gain_ref = bf16[1,512]{1,0:T(2,128)(2,1)} reshape(bf16[512]{0:T(512)(128)(2,1)} %param.24) | data formatting | bytes 2048 | tf_op jit(solution)/shard_map/reshape | solution.py:388
  1.3 24.5 %shard_map.127 = bf16[64,2048]{1,0:T(8,128)(2,1)} custom-call(bf16[128,512]{1,0:T(8,128)(2,1)} %x_ref.1, bf16[128,128]{1,0:T(8,128)(2,1)} %b_ref.1, bf16[128,128]{1,0:T(8,128)(2,1)} %c_ref.1, bf16[128,512]{1,0:T(8,128)(2,1)} %z_hbm.1, bf16[8,128]{1,0:T(8,128)(2,1)} %bitcast.3, f32[8,128]{1,0:T(8,128)} %bitcast.2, bf16[4,512]{1,0:T(4,128)(2,1)} %tx_ref.1, ...), custom_call_target="tpu_custom_call" | custom-call | tf_op jit(solution)/shard_map/pallas_call | solution.py:352
  25.8 1.7 %copy.15 = bf16[64,2048]{1,0:T(8,128)(2,1)} copy(bf16[64,2048]{1,0:T(8,128)(2,1)} %shard_map.127) | data formatting | bytes 524288

commit v2 on v1

--- a/solution.py
+++ b/solution.py
@@ -23,12 +23,13 @@
 
 def kernel(
     n, owners,
-    x_ref, b_ref, c_ref, z_hbm, dt_ref, fade_ref, tx_ref, tb_ref, tc_ref,
-    off_ref, speed_ref, gain_ref, w_hbm,
+    x_hbm, b_hbm, c_hbm, z_hbm, dt_hbm, fade_hbm, tx_hbm, tb_hbm, tc_hbm,
+    off_hbm, speed_hbm, gain_hbm, w_hbm,
     out_ref,
-    z_ref, w_ref, halo_x, halo_b, halo_c, joined, xs, xe, cb, cc, step_e, end_e, grow_e,
-    gate, y_in, dec, dec_in, st, st_in, eb, ent, gg, ssq, ssq_in, p_out, p_in,
-    loc_sem, hs, hr, ds_, dr, s1, r1, s2, r2, sx, rx,
+    x_ref, b_ref, c_ref, z_ref, dt_ref, fade_ref, tx_ref, tb_ref, tc_ref,
+    off_ref, speed_ref, gain_ref, w_ref, halo_x, halo_b, halo_c, joined, xs, xe, cb, cc, step_e, end_e, grow_e,
+    gate, y_in, dec, dec_in, st, st_in, eb, ent, gg, ssq, ssq_in, own, p_out, p_in,
+    loc_sem, know, hs, hr, ds_, dr, s1, r1, s2, r2, sx, rx,
 ):
     length, inner = x_ref.shape
     gw = b_ref.shape[1]
@@ -44,21 +45,65 @@
     core = lax.axis_index("tp")
     mate = 1 - core
 
-    z_copy = pltpu.make_async_copy(z_hbm, z_ref, loc_sem.at[0])
-    w_copy = pltpu.make_async_copy(w_hbm, w_ref, loc_sem.at[1])
-    z_copy.start()
-    w_copy.start()
-
     barrier = pltpu.get_barrier_semaphore()
-
-    def greet(i, carry):
-        pl.semaphore_signal(
-            barrier, inc=1, device_id={"sp": lax.rem(me + i, n)}, device_id_type=MESH
-        )
-        return carry
-
-    lax.fori_loop(1, n, greet, 0)
+    bits = (n - 1).bit_length()
+    for bit in range(bits):
+        other = me + (1 - 2 * lax.rem(me // (1 << bit), 2)) * (1 << bit)
+        pl.semaphore_signal(barrier, inc=1, device_id={"sp": other}, device_id_type=MESH)
     pl.semaphore_signal(barrier, inc=1, device_id={"tp": mate}, device_id_type=MESH)
+
+    @pl.when(me > 0)
+    def _():
+        pl.semaphore_signal(barrier, inc=1, device_id={"sp": me - 1}, device_id_type=MESH)
+
+    @pl.when(me < n - 1)
+    def _():
+        pl.semaphore_signal(barrier, inc=1, device_id={"sp": me + 1}, device_id_type=MESH)
+
+    loads = [
+        pltpu.make_async_copy(src, dst, loc_sem.at[i])
+        for i, (src, dst) in enumerate((
+            (x_hbm, x_ref), (b_hbm, b_ref), (c_hbm, c_ref), (dt_hbm, dt_ref),
+            (fade_hbm, fade_ref), (off_hbm, off_ref), (speed_hbm, speed_ref),
+            (tx_hbm, tx_ref), (tb_hbm, tb_ref), (tc_hbm, tc_ref),
+            (gain_hbm, gain_ref), (z_hbm, z_ref), (w_hbm, w_ref),
+        ))
+    ]
+    for load in loads:
+        load.start()
+
+    edge = halo_x.shape[0]
+    halos = [
+        pltpu.make_async_remote_copy(
+            src_ref=src.at[pl.ds(length - edge, edge)],
+            dst_ref=dst,
+            send_sem=hs.at[i],
+            recv_sem=hr.at[i],
+            device_id={"sp": lax.rem(me + 1, n)},
+            device_id_type=MESH,
+        )
+        for i, (src, dst) in enumerate(((x_ref, halo_x), (b_ref, halo_b), (c_ref, halo_c)))
+    ]
+
+    for load in loads[:10]:
+        load.wait()
+
+    inside = (me > 0).astype(jnp.int32) + (me < n - 1).astype(jnp.int32)
+    pl.semaphore_wait(barrier, bits + 1 + inside)
+
+    @pl.when(me < n - 1)
+    def _():
+        for copy in halos:
+            copy.start()
+
+    def tell(bit):
+        other = me + (1 - 2 * lax.rem(me // (1 << bit), 2)) * (1 << bit)
+        pl.semaphore_signal(know.at[bit], inc=1, device_id={"sp": other}, device_id_type=MESH)
+
+    def hear(bit):
+        pl.semaphore_wait(know.at[bit], 1)
+
+    tell(0)
 
     sub = lax.broadcasted_iota(jnp.int32, (heads, length), 0)
     off = jnp.zeros((heads, length), F32)
@@ -115,25 +160,10 @@
 
     mixed(0, length)
 
-    pl.semaphore_wait(barrier, n)
-
-    edge = halo_x.shape[0]
-    halos = [
-        pltpu.make_async_remote_copy(
-            src_ref=src.at[pl.ds(length - edge, edge)],
-            dst_ref=dst,
-            send_sem=hs.at[i],
-            recv_sem=hr.at[i],
-            device_id={"sp": lax.rem(me + 1, n)},
-            device_id_type=MESH,
-        )
-        for i, (src, dst) in enumerate(((x_ref, halo_x), (b_ref, halo_b), (c_ref, halo_c)))
-    ]
-
-    @pl.when(me < n - 1)
-    def _():
-        for copy in halos:
-            copy.start()
+    for bit in range(bits - 1):
+        hear(bit)
+        if bit + 1 < bits - 1:
+            tell(bit + 1)
 
     base = me // stride
     tile_of = owners // tiles
@@ -233,7 +263,8 @@
                 )
             )
         y_in[:, t * LANES : (t + 1) * LANES] = jnp.where(low_lanes, parts[0], parts[1])
-    z_copy.wait()
+    loads[10].wait()
+    loads[11].wait()
     gate[...] = silu(z_ref[...].astype(F32))
 
     @pl.when(is_owner)
@@ -265,6 +296,7 @@
 
     lax.fori_loop(0, owners, arrive, 0)
 
+    gain = gain_ref[...].astype(F32).reshape(1, inner)
     total = jnp.zeros((length, 1), F32)
     for t in range(tiles):
         g = t // per_group_tiles
@@ -273,7 +305,7 @@
         read = jnp.dot(cc[:, g * STATE : (g + 1) * STATE], held, preferred_element_type=F32)
         gated = (y_in[:, lanes] + grow_e[:, lanes] * read) * gate[:, lanes]
         total += jnp.sum(gated * gated, axis=1, keepdims=True)
-        gg[:, lanes] = (gated * gain_ref[:, lanes].astype(F32)).astype(BF16)
+        gg[:, lanes] = (gated * gain[:, lanes]).astype(BF16)
     ssq[...] = jnp.broadcast_to(total, (length, LANES))
 
     def mate_copy(src, dst, i):
@@ -288,29 +320,25 @@
 
     theirs = pl.ds(pl.multiple_of(mate * half, half), half)
     mine = pl.ds(pl.multiple_of(core * half, half), half)
-    w_copy.wait()
+    first = mate_copy(ssq.at[theirs], ssq_in, chunks)
+    first.start()
+    loads[12].wait()
     sent = []
     for i in range(chunks):
-        p_out[i] = jnp.dot(
-            gg[theirs], w_ref[:, i * cols : (i + 1) * cols], preferred_element_type=F32
-        ).astype(BF16)
-        if i == 0:
-            first = mate_copy(ssq.at[theirs], ssq_in, chunks)
-            first.start()
+        own[i] = jnp.dot(
+            gg[...], w_ref[:, i * cols : (i + 1) * cols], preferred_element_type=F32
+        )
+        p_out[i] = own[i, theirs].astype(BF16)
         copy = mate_copy(p_out.at[i], p_in.at[i], i)
         copy.start()
         sent.append(copy)
-    own = [
-        jnp.dot(gg[mine], w_ref[:, i * cols : (i + 1) * cols], preferred_element_type=F32)
-        for i in range(chunks)
-    ]
     first.wait_recv()
     mean = (ssq[mine] + ssq_in[...]) * (1.0 / (2 * inner))
     scale = lax.rsqrt(mean + EPS)[:, :1]
     for i in range(chunks):
         sent[i].wait_recv()
         out_ref[:, i * cols : (i + 1) * cols] = (
-            (own[i] + p_in[i].astype(F32)) * scale
+            (own[i, mine] + p_in[i].astype(F32)) * scale
         ).astype(BF16)
 
     @pl.when(me < n - 1)
@@ -345,17 +373,27 @@
     chunks = 4
     cols = width // chunks
     vmem = pl.BlockSpec(memory_space=pltpu.VMEM)
-    smem = pl.BlockSpec(memory_space=pltpu.SMEM)
     hbm = pl.BlockSpec(memory_space=pl.ANY)
     V = pltpu.VMEM
     dma = lambda k: pltpu.SemaphoreType.DMA((k,))
     return pl.pallas_call(
         functools.partial(kernel, n, owners),
-        out_shape=jax.ShapeDtypeStruct((half, width), BF16),
-        in_specs=[vmem, vmem, vmem, hbm, vmem, vmem, vmem, vmem, vmem, smem, smem, vmem, hbm],
+        out_shape=pltpu.VMEM((half, width), BF16),
+        in_specs=[hbm] * 13,
         out_specs=vmem,
         scratch_shapes=[
-            V((length, inner), BF16),
+            V(x.shape, BF16),
+            V(b.shape, BF16),
+            V(c.shape, BF16),
+            V(z.shape, BF16),
+            V(dt.shape[::-1], BF16),
+            V(fade.shape[::-1], F32),
+            V(tx.shape, BF16),
+            V(tb.shape, BF16),
+            V(tc.shape, BF16),
+            pltpu.SMEM(off.shape, F32),
+            pltpu.SMEM(speed.shape, F32),
+            V(gain.shape, BF16),
             V(w.shape, BF16),
             V((16, inner), BF16),
             V((16, gw), BF16),
@@ -379,13 +417,14 @@
             V((length, inner), BF16),
             V((length, LANES), F32),
             V((half, LANES), F32),
+            V((chunks, length, cols), F32),
             V((chunks, half, cols), BF16),
             V((chunks, half, cols), BF16),
-            dma(2), dma(3), dma(3), dma(owners), dma(n), dma(owners), dma(n),
+            dma(13), pltpu.SemaphoreType.REGULAR((max(1, (n - 1).bit_length()),)), dma(3), dma(3), dma(owners), dma(n), dma(owners), dma(n),
             dma(n), dma(owners), dma(chunks + 1), dma(chunks + 1),
         ],
         compiler_params=pltpu.CompilerParams(collective_id=0, has_side_effects=True),
-    )(x, b, c, z, dt.T, fade.T, tx, tb, tc, off, speed, gain.reshape(1, inner), w)
+    )(x, b, c, z, dt.T, fade.T, tx, tb, tc, off, speed, gain, w)
 
 
 def solution(mesh):

time: 27.6 us -> 23 us (0.83)
  Pallas kernels: 24.5 us -> 22.1 us
  local copies, waits for them, and re-layouts: 2.93 us -> 0.71 us
    pallas_call x1, Pallas kernels: 24.5 us -> 22.1 us  [per_device(): pl.pallas_call(functools.partial(kernel, n, owners), out_shape=pltpu.VMEM...]
    reshape x1 -> x0, local copies, waits for them, and re-layouts: 1.26 us -> none  [per_device(): gain.reshape(1, inner)]
    unnamed x1, local copies, waits for them, and re-layouts: 1.67 us -> 0.71 us
where the time goes in v2:
time: 23 us; the launch traced here: 22.8 us
  Pallas kernels  22.1 us (96%)
  local copies, waits for them, and re-layouts  0.71 us (3%)
    pallas_call x1, Pallas kernels, per_device(): pl.pallas_call(functools.partial(kernel, n, owners), out_shape=pltpu.VMEM...  22.1 us
    unnamed x1, local copies, waits for them, and re-layouts  0.71 us

profile of v2, /device:TPU:1, one launch (start us, length us, event | category | flops | bytes accessed | tf_op | source)
XLA Modules:
  0.0 22.8 jit_solution(9906119819660130685)
XLA Ops:
  0.0 22.1 %shard_map.127 = bf16[64,2048]{1,0:T(8,128)(2,1)S(1)} custom-call(bf16[128,512]{1,0:T(8,128)(2,1)} %x_hbm.1, bf16[128,128]{1,0:T(8,128)(2,1)} %b_hbm.1, bf16[128,128]{1,0:T(8,128)(2,1)} %c_hbm.1, bf16[128,512]{1,0:T(8,128)(2,1)} %z_hbm.1, bf16[8,128]{1,0:T(8,128)(2,1)} %bitcast.3, f32[8,128]{1,0:T(8,128)} %bitcast.2, bf16[4,512]{1,0:T(4,128)(2,1)} %tx_hbm.1, ...), custom_call_target="tpu_custom_call" | custom-call | tf_op jit(solution)/shard_map/pallas_call | solution.py:379
  22.1 0.7 %copy.15 = bf16[64,2048]{1,0:T(8,128)(2,1)} copy(bf16[64,2048]{1,0:T(8,128)(2,1)S(1)} %shard_map.127) | data formatting | bytes 524288

commit v3 on v2

--- a/solution.py
+++ b/solution.py
@@ -25,18 +25,19 @@
     n, owners,
     x_hbm, b_hbm, c_hbm, z_hbm, dt_hbm, fade_hbm, tx_hbm, tb_hbm, tc_hbm,
     off_hbm, speed_hbm, gain_hbm, w_hbm,
-    out_ref,
-    x_ref, b_ref, c_ref, z_ref, dt_ref, fade_ref, tx_ref, tb_ref, tc_ref,
+    out_hbm,
+    out_ref, x_ref, b_ref, c_ref, z_ref, dt_ref, fade_ref, tx_ref, tb_ref, tc_ref,
     off_ref, speed_ref, gain_ref, w_ref, halo_x, halo_b, halo_c, joined, xs, xe, cb, cc, step_e, end_e, grow_e,
     gate, y_in, dec, dec_in, st, st_in, eb, ent, gg, ssq, ssq_in, own, p_out, p_in,
-    loc_sem, know, hs, hr, ds_, dr, s1, r1, s2, r2, sx, rx,
+    loc_sem, put_sem, know, hs, hr, ds_, dr, s1, r1, s2, r2, sx, rx,
 ):
     length, inner = x_ref.shape
     gw = b_ref.shape[1]
     heads = dt_ref.shape[0]
     tiles = inner // LANES
     per_group_tiles = tiles // (gw // STATE)
-    stride = n // owners
+    front = n // 4
+    stride = (n // 2) // owners
     rows = tiles * STATE // owners
     taps = tx_ref.shape[0]
     half = length // 2
@@ -44,6 +45,7 @@
     me = lax.axis_index("sp")
     core = lax.axis_index("tp")
     mate = 1 - core
+    shifted = lax.rem(me + n - front, n)
 
     barrier = pltpu.get_barrier_semaphore()
     bits = (n - 1).bit_length()
@@ -160,12 +162,16 @@
 
     mixed(0, length)
 
-    for bit in range(bits - 1):
+    for bit in range(bits - 2):
         hear(bit)
-        if bit + 1 < bits - 1:
-            tell(bit + 1)
-
-    base = me // stride
+        tell(bit + 1)
+    middle = shifted < n // 2
+
+    @pl.when(middle)
+    def _():
+        hear(bits - 2)
+
+    base = lax.rem(shifted // stride, owners)
     tile_of = owners // tiles
 
     def dec_copy(owner, slot):
@@ -174,7 +180,7 @@
             dst_ref=dec_in.at[slot],
             send_sem=ds_.at[owner],
             recv_sem=dr.at[slot],
-            device_id={"sp": owner * stride},
+            device_id={"sp": front + owner * stride},
             device_id_type=MESH,
         )
 
@@ -184,7 +190,7 @@
             dst_ref=st_in.at[slot],
             send_sem=s1.at[owner],
             recv_sem=r1.at[slot],
-            device_id={"sp": owner * stride},
+            device_id={"sp": front + owner * stride},
             device_id_type=MESH,
         )
 
@@ -202,7 +208,7 @@
         def body(i, carry):
             owner = lax.rem(base + i, owners)
 
-            @pl.when(owner * stride != me)
+            @pl.when(front + owner * stride != me)
             def _():
                 getattr(make(owner, slot), method)()
 
@@ -210,7 +216,7 @@
 
         lax.fori_loop(0, owners, body, 0)
 
-    is_owner = lax.rem(me, stride) == 0
+    is_owner = (shifted < n // 2) & (lax.rem(shifted, stride) == 0)
     to_owners(dec_copy, "start", me)
 
     @pl.when(is_owner)
@@ -281,20 +287,35 @@
         lax.fori_loop(0, n, turn, jnp.zeros((rows, LANES), F32))
 
         def deliver(i, carry):
-            ent_copy(lax.rem(me + i, n), base).start()
+            place = lax.rem(me + i, n)
+
+            @pl.when(place > 0)
+            def _():
+                ent_copy(place, base).start()
+
             return carry
 
         lax.fori_loop(1, n, deliver, 0)
         ent[base] = eb[me]
 
+    @pl.when(jnp.logical_not(middle))
+    def _():
+        hear(bits - 2)
+
+    @pl.when(me == 0)
+    def _():
+        ent[...] = jnp.zeros_like(ent)
+
     def arrive(owner, carry):
-        @pl.when(owner * stride != me)
+        @pl.when(front + owner * stride != me)
         def _():
             ent_copy(me, owner).wait_recv()
 
         return carry
 
-    lax.fori_loop(0, owners, arrive, 0)
+    @pl.when(me > 0)
+    def _():
+        lax.fori_loop(0, owners, arrive, 0)
 
     gain = gain_ref[...].astype(F32).reshape(1, inner)
     total = jnp.zeros((length, 1), F32)
@@ -335,11 +356,19 @@
     first.wait_recv()
     mean = (ssq[mine] + ssq_in[...]) * (1.0 / (2 * inner))
     scale = lax.rsqrt(mean + EPS)[:, :1]
+    puts = []
     for i in range(chunks):
         sent[i].wait_recv()
         out_ref[:, i * cols : (i + 1) * cols] = (
             (own[i, mine] + p_in[i].astype(F32)) * scale
         ).astype(BF16)
+        put = pltpu.make_async_copy(
+            out_ref.at[:, i * cols : (i + 1) * cols],
+            out_hbm.at[:, i * cols : (i + 1) * cols],
+            put_sem.at[i],
+        )
+        put.start()
+        puts.append(put)
 
     @pl.when(me < n - 1)
     def _():
@@ -352,7 +381,12 @@
     @pl.when(is_owner)
     def _():
         def sent_one(i, carry):
-            ent_copy(lax.rem(me + i, n), base).wait_send()
+            place = lax.rem(me + i, n)
+
+            @pl.when(place > 0)
+            def _():
+                ent_copy(place, base).wait_send()
+
             return carry
 
         lax.fori_loop(1, n, sent_one, 0)
@@ -360,6 +394,8 @@
     first.wait_send()
     for copy in sent:
         copy.wait_send()
+    for put in puts:
+        put.wait()
 
 
 def per_device(n, x, b, c, z, dt, fade, tx, tb, tc, off, speed, gain, w):
@@ -367,7 +403,7 @@
     gw = b.shape[1]
     width = w.shape[1]
     tiles = inner // LANES
-    owners = min(n, tiles * STATE // 16)
+    owners = min(n // 2, tiles * STATE // 16)
     rows = tiles * STATE // owners
     half = length // 2
     chunks = 4
@@ -380,8 +416,9 @@
         functools.partial(kernel, n, owners),
         out_shape=pltpu.VMEM((half, width), BF16),
         in_specs=[hbm] * 13,
-        out_specs=vmem,
+        out_specs=hbm,
         scratch_shapes=[
+            V((half, width), BF16),
             V(x.shape, BF16),
             V(b.shape, BF16),
             V(c.shape, BF16),
@@ -420,7 +457,7 @@
             V((chunks, length, cols), F32),
             V((chunks, half, cols), BF16),
             V((chunks, half, cols), BF16),
-            dma(13), pltpu.SemaphoreType.REGULAR((max(1, (n - 1).bit_length()),)), dma(3), dma(3), dma(owners), dma(n), dma(owners), dma(n),
+            dma(13), dma(chunks), pltpu.SemaphoreType.REGULAR((max(1, (n - 1).bit_length()),)), dma(3), dma(3), dma(owners), dma(n), dma(owners), dma(n),
             dma(n), dma(owners), dma(chunks + 1), dma(chunks + 1),
         ],
         compiler_params=pltpu.CompilerParams(collective_id=0, has_side_effects=True),

time: 23 us -> 20.4 us (0.89)
  the two profiles are of different devices: /device:TPU:1 before, /device:TPU:9 now
where the time goes in v3:
time: 20.4 us; the launch traced here: 20.3 us
  Pallas kernels  19.6 us (96%)
  local copies, waits for them, and re-layouts  0.71 us (3%)
    pallas_call x1, Pallas kernels, per_device(): pl.pallas_call(functools.partial(kernel, n, owners), out_shape=pltpu.VMEM...  19.6 us
    unnamed x1, local copies, waits for them, and re-layouts  0.71 us

profile of v3, /device:TPU:9, one launch (start us, length us, event | category | flops | bytes accessed | tf_op | source)
XLA Modules:
  0.0 20.3 jit_solution(14506019396103946013)
XLA Ops:
  0.0 19.6 %shard_map.127 = bf16[64,2048]{1,0:T(8,128)(2,1)S(1)} custom-call(bf16[128,512]{1,0:T(8,128)(2,1)} %x_hbm.1, bf16[128,128]{1,0:T(8,128)(2,1)} %b_hbm.1, bf16[128,128]{1,0:T(8,128)(2,1)} %c_hbm.1, bf16[128,512]{1,0:T(8,128)(2,1)} %z_hbm.1, bf16[8,128]{1,0:T(8,128)(2,1)} %bitcast.3, f32[8,128]{1,0:T(8,128)} %bitcast.2, bf16[4,512]{1,0:T(4,128)(2,1)} %tx_hbm.1, ...), custom_call_target="tpu_custom_call" | custom-call | tf_op jit(solution)/shard_map/pallas_call | solution.py:415
  19.6 0.7 %copy.15 = bf16[64,2048]{1,0:T(8,128)(2,1)} copy(bf16[64,2048]{1,0:T(8,128)(2,1)S(1)} %shard_map.127) | data formatting | bytes 524288

commit v4 on v3

--- a/solution.py
+++ b/solution.py
@@ -178,8 +178,8 @@
         return pltpu.make_async_remote_copy(
             src_ref=dec.at[owner // tile_of],
             dst_ref=dec_in.at[slot],
-            send_sem=ds_.at[owner],
-            recv_sem=dr.at[slot],
+            send_sem=ds_.at[0],
+            recv_sem=dr.at[0],
             device_id={"sp": front + owner * stride},
             device_id_type=MESH,
         )
@@ -188,8 +188,8 @@
         return pltpu.make_async_remote_copy(
             src_ref=st.at[owner],
             dst_ref=st_in.at[slot],
-            send_sem=s1.at[owner],
-            recv_sem=r1.at[slot],
+            send_sem=s1.at[0],
+            recv_sem=r1.at[0],
             device_id={"sp": front + owner * stride},
             device_id_type=MESH,
         )
@@ -198,11 +198,22 @@
         return pltpu.make_async_remote_copy(
             src_ref=eb.at[place],
             dst_ref=ent.at[slot],
-            send_sem=s2.at[place],
-            recv_sem=r2.at[slot],
+            send_sem=s2.at[0],
+            recv_sem=r2.at[0],
             device_id={"sp": place},
             device_id_type=MESH,
         )
+
+    def drained(ref, count, sem, method):
+        part = ref.at[pl.ds(0, count)]
+        getattr(pltpu.make_async_remote_copy(
+            src_ref=part,
+            dst_ref=part,
+            send_sem=sem.at[0],
+            recv_sem=sem.at[0],
+            device_id={"tp": mate},
+            device_id_type=MESH,
+        ), method)()
 
     def to_owners(make, method, slot):
         def body(i, carry):
@@ -275,12 +286,10 @@
 
     @pl.when(is_owner)
     def _():
+        drained(dec_in, n - 1, dr, "wait_recv")
+        drained(st_in, n - 1, r1, "wait_recv")
+
         def turn(k, state):
-            @pl.when(k != me)
-            def _():
-                dec_copy(base, k).wait_recv()
-                st_copy(base, k).wait_recv()
-
             eb[k] = state.astype(BF16)
             return dec_in[k] * state + st_in[k].astype(F32)
 
@@ -306,16 +315,13 @@
     def _():
         ent[...] = jnp.zeros_like(ent)
 
-    def arrive(owner, carry):
-        @pl.when(front + owner * stride != me)
-        def _():
-            ent_copy(me, owner).wait_recv()
-
-        return carry
-
-    @pl.when(me > 0)
-    def _():
-        lax.fori_loop(0, owners, arrive, 0)
+    @pl.when((me > 0) & jnp.logical_not(is_owner))
+    def _():
+        drained(ent, owners, r2, "wait_recv")
+
+    @pl.when(is_owner)
+    def _():
+        drained(ent, owners - 1, r2, "wait_recv")
 
     gain = gain_ref[...].astype(F32).reshape(1, inner)
     total = jnp.zeros((length, 1), F32)
@@ -375,21 +381,16 @@
         for copy in halos:
             copy.wait_send()
 
-    to_owners(dec_copy, "wait_send", me)
-    to_owners(st_copy, "wait_send", me)
+    @pl.when(jnp.logical_not(is_owner))
+    def _():
+        drained(dec_in, owners, ds_, "wait_send")
+        drained(st, owners, s1, "wait_send")
 
     @pl.when(is_owner)
     def _():
-        def sent_one(i, carry):
-            place = lax.rem(me + i, n)
-
-            @pl.when(place > 0)
-            def _():
-                ent_copy(place, base).wait_send()
-
-            return carry
-
-        lax.fori_loop(1, n, sent_one, 0)
+        drained(dec_in, owners - 1, ds_, "wait_send")
+        drained(st, owners - 1, s1, "wait_send")
+        drained(eb, n - 2, s2, "wait_send")
 
     first.wait_send()
     for copy in sent:
@@ -457,8 +458,8 @@
             V((chunks, length, cols), F32),
             V((chunks, half, cols), BF16),
             V((chunks, half, cols), BF16),
-            dma(13), dma(chunks), pltpu.SemaphoreType.REGULAR((max(1, (n - 1).bit_length()),)), dma(3), dma(3), dma(owners), dma(n), dma(owners), dma(n),
-            dma(n), dma(owners), dma(chunks + 1), dma(chunks + 1),
+            dma(13), dma(chunks), pltpu.SemaphoreType.REGULAR((max(1, (n - 1).bit_length()),)), dma(3), dma(3), dma(1), dma(1), dma(1), dma(1),
+            dma(1), dma(1), dma(chunks + 1), dma(chunks + 1),
         ],
         compiler_params=pltpu.CompilerParams(collective_id=0, has_side_effects=True),
     )(x, b, c, z, dt.T, fade.T, tx, tb, tc, off, speed, gain, w)

time: 20.4 us -> 19.6 us (0.961)
  the two profiles are of different devices: /device:TPU:9 before, /device:TPU:5 now
where the time goes in v4:
time: 19.6 us; the launch traced here: 19.5 us
  Pallas kernels  18.8 us (96%)
  local copies, waits for them, and re-layouts  0.71 us (4%)
    pallas_call x1, Pallas kernels, per_device(): pl.pallas_call(functools.partial(kernel, n, owners), out_shape=pltpu.VMEM...  18.8 us
    unnamed x1, local copies, waits for them, and re-layouts  0.71 us

profile of v4, /device:TPU:5, one launch (start us, length us, event | category | flops | bytes accessed | tf_op | source)
XLA Modules:
  0.0 19.5 jit_solution(6777638439117193775)
XLA Ops:
  0.0 18.8 %shard_map.127 = bf16[64,2048]{1,0:T(8,128)(2,1)S(1)} custom-call(bf16[128,512]{1,0:T(8,128)(2,1)} %x_hbm.1, bf16[128,128]{1,0:T(8,128)(2,1)} %b_hbm.1, bf16[128,128]{1,0:T(8,128)(2,1)} %c_hbm.1, bf16[128,512]{1,0:T(8,128)(2,1)} %z_hbm.1, bf16[8,128]{1,0:T(8,128)(2,1)} %bitcast.3, f32[8,128]{1,0:T(8,128)} %bitcast.2, bf16[4,512]{1,0:T(4,128)(2,1)} %tx_hbm.1, ...), custom_call_target="tpu_custom_call" | custom-call | tf_op jit(solution)/shard_map/pallas_call | solution.py:416
  18.8 0.7 %copy.15 = bf16[64,2048]{1,0:T(8,128)(2,1)} copy(bf16[64,2048]{1,0:T(8,128)(2,1)S(1)} %shard_map.127) | data formatting | bytes 524288
